TPU v7x, 32 devices: a whole 2x2x4 slice. The times are simulated.
32 devices in a mesh: sp: 32 (over z, y, x, core), tp: 1.
Axes of the slice: x: 2, y: 2, z: 4, core: 2. Of those that a mesh axis runs over, the one named last changes fastest.
Arguments:
- queries: bfloat16 [8192, 1024], P('sp', 'tp'), may hold values from -30 to 30
- keys: bfloat16 [8192, 256], P('sp', 'tp'), may hold values from -30 to 30
- values: bfloat16 [8192, 256], P('sp', 'tp'), may hold values from -20 to 20
- gate_totals: float32 [8192, 16], P('sp', 'tp'), may hold values from -8192 to 0, as said below
- documents: int32 [8192], P('sp'), may hold values from 0 to 1, never falling along the last dimension, each value on 1 to 6144 neighbouring positions
- stream: bfloat16 [8192, 2048], P(('sp', 'tp')), may hold values from -3 to 3
- out_weight: bfloat16 [1024, 2048], replicated, may hold values from -0.1875 to 0.1875
- norm_gain: float32 [2048], replicated, may hold values from 0.1 to 1.9
- routes: int32 [8192, 2], P(('sp', 'tp')), may hold values from 0 to 31, all different within a row; in each aligned block of 256 rows (0 to 255, 256 to 511, ...) at most 32 rows name the same one
- route_weights: float32 [8192, 2], P(('sp', 'tp')), may hold values from 0.2 to 1
- expert_gate: bfloat16 [32, 2048, 1024], P('sp', None, 'tp'), may hold values from -0.125 to 0.125
- expert_up: bfloat16 [32, 2048, 1024], P('sp', None, 'tp'), may hold values from -0.125 to 0.125
- expert_down: bfloat16 [32, 1024, 2048], P('sp', 'tp'), may hold values from -0.1875 to 0.1875
Outputs:
- output: bfloat16 [8192, 2048], P(('sp', 'tp'))
Inputs may be any that keep to these rules, and one draw needn't show every extreme that they name: `gate_totals`: along positions it never rises, for every head. `routes`: in each aligned block of rows held by one device, no expert is named by more than 32 rows.
All inputs are finite; a program needn't handle non-finite values.
Results may differ from a plain program's by a relative error of at most 0.014.
Values may be sent and summed in bfloat16 or wider, within the bound.
A program may use at most 128 MiB of HBM per device.

v0:
```python
import functools
import math

import jax
import jax.numpy as jnp
from jax import lax
from jax.experimental import pallas as pl
from jax.experimental.pallas import tpu as pltpu
from jax.sharding import PartitionSpec as P

QUERY_HEAD_COUNT = 16
KV_HEADS = 4
HD = 64
TOP = 2


EPS = 1e-06
MASKED = -1e30


def make_fold(query_rows, query_gate, key_gate_all, query_docs, first_pos, kv_local, group):
    count = query_rows.shape[0]
    scale = HD ** (-0.5)
    query_blk = query_rows.reshape(count, kv_local, group, HD)
    gate_here = query_gate.T.reshape(kv_local, group, count, 1)
    query_pos = first_pos + jnp.arange(count, dtype=jnp.int32)
    last_pos = first_pos + count - 1
    first_doc = query_docs[0]

    def block_step(carry, block_in):
        running_max, running_sum, carried = carry
        key_block, value_block, doc_block, pos_block = block_in
        width = key_block.shape[0]

        def compute(unused):
            key_heads = key_block.reshape(width, kv_local, HD)
            value_heads = value_block.reshape(width, kv_local, HD)
            gate_keys = lax.dynamic_slice_in_dim(key_gate_all, pos_block[0], width, 0).T.reshape(
                kv_local, group, 1, width
            )
            scores = (
                jnp.einsum(
                    "qkgd,nkd->kgqn", query_blk, key_heads, preferred_element_type=jnp.float32
                )
                * scale
                + gate_here
                - gate_keys
            )
            allowed = (pos_block[None, :] <= query_pos[:, None]) & (
                doc_block[None, :] == query_docs[:, None]
            )
            scores = jnp.where(allowed, scores, MASKED)
            new_max = jnp.maximum(running_max, jnp.max(scores, axis=-1))
            weights = jnp.where(allowed, jnp.exp(scores - new_max[..., None]), 0.0)
            factor = jnp.exp(running_max - new_max)
            new_sum = running_sum * factor + jnp.sum(weights, axis=-1)
            new_carried = carried * factor[..., None] + jnp.einsum(
                "kgqn,nkd->kgqd",
                weights.astype(jnp.bfloat16),
                value_heads,
                preferred_element_type=jnp.float32,
            )
            return (new_max, new_sum, new_carried)

        skipped = (pos_block[0] > last_pos) | (doc_block[width - 1] < first_doc)
        return (lax.cond(skipped, lambda unused: carry, compute, 0), None)

    def fold(carry, piece, start):
        key_piece, value_piece, doc_piece = piece
        length = key_piece.shape[0]
        width = math.gcd(length, 512)
        blocks_count = length // width
        pos_piece = jnp.arange(length, dtype=jnp.int32)
        blocks = (
            key_piece.reshape(blocks_count, width, -1),
            value_piece.reshape(blocks_count, width, -1),
            doc_piece.reshape(blocks_count, width),
            pos_piece.reshape(blocks_count, width),
        )
        carry, unused = lax.scan(block_step, carry, blocks)
        return carry

    initial = (
        jnp.full((kv_local, group, count), MASKED, jnp.float32),
        jnp.zeros((kv_local, group, count), jnp.float32),
        jnp.zeros((kv_local, group, count, HD), jnp.float32),
    )
    return (fold, initial)


def finish(running_sum, carried):
    mixed = carried / running_sum[..., None]
    count = mixed.shape[2]
    return jnp.transpose(mixed, (2, 0, 1, 3)).reshape(count, -1).astype(jnp.bfloat16)


def shards(
    queries,
    keys,
    values,
    gate_totals,
    documents,
    stream,
    out_weight,
    norm_gain,
    routes,
    route_weights,
    expert_gate,
    expert_up,
    expert_down,
):
    tp_count = lax.axis_size("tp")
    sp_count = lax.axis_size("sp")
    tp_index = lax.axis_index("tp")
    sp_index = lax.axis_index("sp")
    group = QUERY_HEAD_COUNT // KV_HEADS
    tok_local = queries.shape[0]
    own_rows = tok_local // tp_count
    first_row = sp_index * tok_local
    query_rows = lax.all_to_all(queries, "tp", split_axis=0, concat_axis=1, tiled=True)
    key_whole, value_whole = (
        lax.all_gather(keys, "tp", axis=1, tiled=True),
        lax.all_gather(values, "tp", axis=1, tiled=True),
    )
    gate_whole = lax.all_gather(gate_totals, "tp", axis=1, tiled=True)
    key_gate_all = lax.all_gather(gate_whole, "sp", axis=0, tiled=True)
    query_gate = lax.dynamic_slice_in_dim(gate_whole, tp_index * own_rows, own_rows, 0)
    query_docs = lax.dynamic_slice_in_dim(documents, tp_index * own_rows, own_rows, 0)
    fold, initial = make_fold(
        query_rows,
        query_gate,
        key_gate_all,
        query_docs,
        first_row + tp_index * own_rows,
        KV_HEADS,
        group,
    )
    running_max, running_sum, carried = fold(
        initial,
        (
            lax.all_gather(key_whole, "sp", axis=0, tiled=True),
            lax.all_gather(value_whole, "sp", axis=0, tiled=True),
            lax.all_gather(documents, "sp", axis=0, tiled=True),
        ),
        jnp.int32(0),
    )
    attended = finish(running_sum, carried)
    hidden = (
        stream.astype(jnp.float32)
        + jnp.dot(attended, out_weight, preferred_element_type=jnp.float32)
    ).astype(jnp.bfloat16)
    hidden_f = hidden.astype(jnp.float32)
    normed = (
        hidden_f
        * lax.rsqrt(jnp.mean(hidden_f * hidden_f, axis=-1, keepdims=True) + EPS)
        * norm_gain
    ).astype(jnp.bfloat16)
    local_experts = expert_gate.shape[0]
    experts_total = local_experts * sp_count
    capacity = max(2, 2 * tok_local * TOP // (tp_count * experts_total))
    flat = routes.reshape(-1)
    hits = (flat[:, None] == jnp.arange(experts_total, dtype=jnp.int32)[None, :]).astype(jnp.int32)
    slot_index = jnp.sum(jnp.cumsum(hits, axis=0) * hits, axis=1) - 1
    target = flat * capacity + slot_index
    entry_rows = jnp.repeat(normed, TOP, axis=0)
    outgoing = (
        jnp.zeros((experts_total * capacity, normed.shape[1]), jnp.bfloat16)
        .at[target]
        .set(entry_rows)
    )
    outgoing = outgoing.reshape(experts_total, capacity, -1)
    arrived = lax.all_to_all(outgoing, "sp", split_axis=0, concat_axis=0, tiled=True)
    slots = arrived.shape[1]
    both_halves = lax.all_gather(arrived, "tp", axis=0, tiled=True)
    grouped = both_halves.reshape(tp_count * sp_count, local_experts, slots, -1)
    gate = jnp.einsum("secd,edf->secf", grouped, expert_gate, preferred_element_type=jnp.float32)
    upper = jnp.einsum("secd,edf->secf", grouped, expert_up, preferred_element_type=jnp.float32)
    inner = (jax.nn.silu(gate) * upper).astype(jnp.bfloat16)
    partial_value = jnp.einsum(
        "secf,efd->secd", inner, expert_down, preferred_element_type=jnp.float32
    )
    partial_value = lax.optimization_barrier(partial_value.astype(jnp.bfloat16)).astype(jnp.float32)
    summed = lax.psum_scatter(
        partial_value.reshape(tp_count * sp_count * local_experts, slots, -1).astype(jnp.bfloat16),
        "tp",
        scatter_dimension=0,
        tiled=True,
    )
    returned = lax.all_to_all(summed, "sp", split_axis=0, concat_axis=0, tiled=True)
    answers = returned.reshape(experts_total * capacity, -1)[target].reshape(own_rows, TOP, -1)
    routed = jnp.sum(route_weights[..., None] * answers.astype(jnp.float32), axis=1)
    return (hidden_f + routed).astype(jnp.bfloat16)


def attend_kernel(sub, span, width, boundary_ref, query_ref, kv_ref, gate_ref, out_ref):
    tile = pl.program_id(0)
    stripes = kv_ref.shape[0]
    stripe = lax.rem(lax.axis_index("sp"), stripes)
    blocks = query_ref.shape[0]
    block = span // blocks
    group = QUERY_HEAD_COUNT // KV_HEADS
    rows = blocks * sub
    boundary = boundary_ref[0]
    first = tile * span
    per_tile = span // width
    taken = width // block
    zeros = jnp.zeros((rows, HD), jnp.bfloat16)
    query = query_ref[...].reshape(rows, group * HD) * jnp.bfloat16(HD ** (-0.5))
    stacked = jnp.concatenate(
        [
            jnp.concatenate([query[:, head * HD:(head + 1) * HD], zeros], axis=1)
            for head in range(group)
        ],
        axis=0,
    )
    row = lax.broadcasted_iota(jnp.int32, (rows, 1), 0)
    query_pos = first + (row // sub) * block + stripe * sub + lax.rem(row, sub)
    doc_start = jnp.where(query_pos >= boundary, boundary, 0)
    origin = gate_ref[tile * per_tile][:, :, 0:1]
    lane = lax.broadcasted_iota(jnp.int32, (width, 2 * HD), 1)

    def chunk(index, carry, masked):
        per_z = stripes // taken
        kv = kv_ref[pl.ds(lax.rem(index, per_z) * taken, taken), index // per_z, 0:block, :]
        kv = kv.reshape(width, 2 * HD)
        bias = origin - gate_ref[index]
        if masked:
            key_pos = index * width + lax.broadcasted_iota(jnp.int32, (1, width), 1)
            allowed = (key_pos <= query_pos) & (key_pos >= doc_start)
        scores = lax.dot_general(
            stacked, kv, (((1,), (1,)), ((), ())), preferred_element_type=jnp.float32
        )
        tops, mixed = carry
        new_tops, factors, weights = [], [], []
        for head in range(group):
            score = scores[head * rows:(head + 1) * rows] + bias[head]
            if masked:
                score = jnp.where(allowed, score, MASKED)
            new_top = jnp.maximum(tops[head], jnp.max(score, axis=1, keepdims=True))
            weight = jnp.exp(score - new_top)
            factor = jnp.exp(tops[head] - new_top)
            new_tops.append(new_top)
            factors.append(factor)
            weights.append(weight.astype(jnp.bfloat16))
        mixed = mixed * jnp.concatenate(factors, axis=0) + jnp.dot(
            jnp.concatenate(weights, axis=0),
            jnp.where(lane < HD, jnp.bfloat16(1), kv),
            preferred_element_type=jnp.float32,
        )
        return (tuple(new_tops), mixed)

    carry = (
        tuple(jnp.full((rows, 1), 0.5 * MASKED, jnp.float32) for unused in range(group)),
        jnp.zeros((group * rows, 2 * HD), jnp.float32),
    )
    own = tile * per_tile
    inside = (boundary > first) & (boundary < first + span)
    second = first >= boundary
    low = jnp.where(second, boundary // width, 0)
    clean_low = jnp.where(inside, own, jnp.where(second, (boundary + width - 1) // width, 0))
    clean_low = jnp.minimum(clean_low, own)
    carry = lax.fori_loop(low, clean_low, lambda i, c: chunk(i, c, True), carry)
    carry = lax.fori_loop(clean_low, own, lambda i, c: chunk(i, c, False), carry)
    carry = lax.fori_loop(own, own + per_tile, lambda i, c: chunk(i, c, True), carry)
    unused, mixed = carry
    ratio = mixed[:, HD:] / mixed[:, :HD]
    parts = [ratio[head * rows:(head + 1) * rows] for head in range(group)]
    out_ref[...] = jnp.concatenate(parts, axis=1).astype(jnp.bfloat16).reshape(out_ref.shape)


def fast_shards(
    queries,
    keys,
    values,
    gate_totals,
    documents,
    stream,
    out_weight,
    norm_gain,
    routes,
    route_weights,
    expert_gate,
    expert_up,
    expert_down,
):
    sp_count = lax.axis_size("sp")
    group = QUERY_HEAD_COUNT // KV_HEADS
    tok = queries.shape[0]
    stripes = sp_count // KV_HEADS
    sub = tok // stripes
    blocks = 4
    span = blocks * tok
    width = min(span, 1024)
    tiles = sp_count // blocks
    lanes = 2 * HD
    part_a = lax.reduce_precision(gate_totals, 8, 7)
    rest = gate_totals - part_a
    part_b = lax.reduce_precision(rest, 8, 7)
    part_c = rest - part_b
    parts = jnp.stack([part_a, part_b, part_c], axis=0).astype(jnp.bfloat16)
    parts = jnp.transpose(parts.reshape(3, tok, KV_HEADS, group), (2, 0, 3, 1))
    parts = parts.reshape(KV_HEADS, 3 * group, tok)
    docs = jnp.broadcast_to(documents.astype(jnp.bfloat16)[None, None, :], (KV_HEADS, 4, tok))
    extra = jnp.concatenate([parts, docs], axis=1).reshape(KV_HEADS, -1, lanes)
    kv = jnp.concatenate(
        [keys.reshape(tok, KV_HEADS, HD), values.reshape(tok, KV_HEADS, HD)], axis=2
    )
    message = jnp.concatenate([jnp.transpose(kv, (1, 0, 2)), extra], axis=1)
    across = [[g * stripes + j for g in range(KV_HEADS)] for j in range(stripes)]
    within = [[g * stripes + j for j in range(stripes)] for g in range(KV_HEADS)]
    column = lax.all_to_all(
        message, "sp", split_axis=0, concat_axis=0, axis_index_groups=across, tiled=True
    )
    kv_all = lax.all_to_all(
        jnp.broadcast_to(column[None], (stripes,) + column.shape),
        "sp",
        split_axis=0,
        concat_axis=0,
        axis_index_groups=within,
        tiled=True,
    )
    query_send = jnp.transpose(
        queries.reshape(stripes, sub, KV_HEADS, group * HD), (2, 0, 1, 3)
    ).reshape(sp_count, sub, group * HD)
    query_got = lax.all_to_all(query_send, "sp", split_axis=0, concat_axis=0, tiled=True)
    extra_all = jnp.transpose(kv_all[:, :, tok:, :], (1, 0, 2, 3)).reshape(sp_count, 16, tok)
    extra_all = extra_all.astype(jnp.float32)
    boundary = jnp.sum((extra_all[:, 3 * group, :] < 0.5).astype(jnp.int32)).reshape(1)
    gates = extra_all[:, :group] + extra_all[:, group:2 * group] + extra_all[:, 2 * group:3 * group]
    gates = jnp.transpose(gates.reshape(tiles, blocks, group, tok), (0, 2, 1, 3))
    gates = jnp.transpose(gates.reshape(tiles, group, span // width, 1, width), (0, 2, 1, 3, 4))
    gates = gates.reshape(-1, group, 1, width)
    mixed = pl.pallas_call(
        functools.partial(attend_kernel, sub, span, width),
        grid=(tiles,),
        in_specs=[
            pl.BlockSpec(memory_space=pltpu.SMEM),
            pl.BlockSpec((blocks, sub, group * HD), lambda i: (i, 0, 0)),
            pl.BlockSpec(kv_all.shape, lambda i: (0, 0, 0, 0)),
            pl.BlockSpec(gates.shape, lambda i: (0, 0, 0, 0)),
        ],
        out_specs=pl.BlockSpec((blocks, sub, group * HD), lambda i: (i, 0, 0)),
        out_shape=jax.ShapeDtypeStruct((sp_count, sub, group * HD), jnp.bfloat16),
        compiler_params=pltpu.CompilerParams(vmem_limit_bytes=48 * 1024 * 1024),
        name="attend",
    )(boundary, query_got, kv_all, gates)
    back = lax.all_to_all(mixed, "sp", split_axis=0, concat_axis=0, tiled=True)
    attended = jnp.transpose(
        back.reshape(KV_HEADS, stripes, sub, group * HD), (1, 2, 0, 3)
    ).reshape(tok, QUERY_HEAD_COUNT * HD)
    hidden = (
        stream.astype(jnp.float32)
        + jnp.dot(attended, out_weight, preferred_element_type=jnp.float32)
    ).astype(jnp.bfloat16)
    hidden_f = hidden.astype(jnp.float32)
    normed = (
        hidden_f
        * lax.rsqrt(jnp.mean(hidden_f * hidden_f, axis=-1, keepdims=True) + EPS)
        * norm_gain
    ).astype(jnp.bfloat16)
    experts_total = sp_count
    capacity = max(2, 2 * tok * TOP // experts_total)
    slots = experts_total * capacity
    flat = routes.reshape(-1)
    hits = (flat[:, None] == jnp.arange(experts_total, dtype=jnp.int32)[None, :]).astype(jnp.int32)
    slot_index = jnp.sum(jnp.cumsum(hits, axis=0) * hits, axis=1) - 1
    target = (flat * capacity + slot_index).reshape(tok, TOP)
    line = jnp.arange(slots, dtype=jnp.int32)
    placed = sum(
        (line[:, None] == target[:, k][None, :]).astype(jnp.bfloat16) for k in range(TOP)
    )
    outgoing = jnp.dot(placed, normed, preferred_element_type=jnp.float32).astype(jnp.bfloat16)
    arrived = lax.all_to_all(
        outgoing.reshape(experts_total, capacity, -1), "sp", split_axis=0, concat_axis=0, tiled=True
    ).reshape(slots, -1)
    gate = jnp.dot(arrived, expert_gate[0], preferred_element_type=jnp.float32)
    upper = jnp.dot(arrived, expert_up[0], preferred_element_type=jnp.float32)
    inner = (jax.nn.silu(gate) * upper).astype(jnp.bfloat16)
    answer = jnp.dot(inner, expert_down[0], preferred_element_type=jnp.float32).astype(jnp.bfloat16)
    returned = lax.all_to_all(
        answer.reshape(sp_count, capacity, -1), "sp", split_axis=0, concat_axis=0, tiled=True
    ).reshape(slots, -1)
    share = sum(
        jnp.where(line[None, :] == target[:, k][:, None], route_weights[:, k][:, None], 0.0)
        for k in range(TOP)
    )
    share_high = lax.reduce_precision(share, 8, 7)
    share_low = (share - share_high).astype(jnp.bfloat16)
    routed = jnp.dot(
        share_high.astype(jnp.bfloat16), returned, preferred_element_type=jnp.float32
    ) + jnp.dot(share_low, returned, preferred_element_type=jnp.float32)
    return (hidden_f + routed).astype(jnp.bfloat16)


def solution(mesh):
    sp_count, tp_count = mesh.shape["sp"], mesh.shape["tp"]
    fast = tp_count == 1 and sp_count % 32 == 0
    return jax.shard_map(
        fast_shards if fast else shards,
        mesh=mesh,
        in_specs=(
            P("sp", "tp"),
            P("sp", "tp"),
            P("sp", "tp"),
            P("sp", "tp"),
            P("sp"),
            P(("sp", "tp"), None),
            P(),
            P(),
            P(("sp", "tp"), None),
            P(("sp", "tp"), None),
            P("sp", None, "tp"),
            P("sp", None, "tp"),
            P("sp", "tp", None),
        ),
        out_specs=P(("sp", "tp"), None),
        check_vma=False,
    )
```

profile of v0, /device:TPU:19, one launch (start us, length us, event | category | flops | bytes accessed | tf_op | source)
XLA Modules:
  0.0 342.0 jit_solution(17490617531177138348)
XLA Ops:
  0.0 0.7 reduce-precision_convert_fusion.3
  0.8 0.7 convert_element_type.60
  1.7 1.0 copy.66
  2.7 1.0 copy.67
  3.8 0.2 copy.73
  4.1 11.6 %all_to_all.30 = bf16[4,288,128]{2,1,0:T(8,128)(2,1)S(1)} all-to-all(bf16[4,288,128]{2,1,0:T(8,128)(2,1)S(1)} %copy.73), channel_id=1, replica_groups={{0,8,16,24},{1,9,17,25},{2,10,18,26},{3,11,19,27},{4,12,20,28},{5,13,21..., dimensions={0} | all-to-all | bytes 589824 | tf_op jit(solution)/shard_map/all_to_all | solution.py:311
  15.7 1.8 broadcast_in_dim.42
  17.5 5.2 %all-to-all-start.1 = ((bf16[8,4,288,128]{3,2,1,0:T(8,128)(2,1)}), bf16[8,4,288,128]{3,2,1,0:T(8,128)(2,1)S(1)}, u32[]{:S(2)}, u32[]{:S(2)}) async-start(bf16[8,4,288,128]{3,2,1,0:T(8,128)(2,1)} %broadcast_in_dim.42), calls=%async_computation.1 | async-start | bytes 4718592 | tf_op jit(solution)/shard_map/all_to_all | solution.py:314
  22.7 0.4 reshape.98
  23.0 0.9 copy.75
  24.0 26.6 %all-to-all-done.1.kv_ref = bf16[8,4,288,128]{3,2,1,0:T(8,128)(2,1)S(1)} async-done(((bf16[8,4,288,128]{3,2,1,0:T(8,128)(2,1)}), bf16[8,4,288,128]{3,2,1,0:T(8,128)(2,1)S(1)}, u32[]{:S(2)}, u32[]{:S(2)}) %all-to-all-start.1) | async-done | bytes 2359328 | tf_op jit(solution)/shard_map/all_to_all | solution.py:314
  50.5 5.8 %all-to-all-start.2 = ((bf16[32,32,256]{2,1,0:T(8,128)(2,1)}), bf16[32,32,256]{2,1,0:T(8,128)(2,1)S(1)}, u32[]{:S(2)}, u32[]{:S(2)}) async-start(bf16[32,32,256]{2,1,0:T(8,128)(2,1)} %bitcast.8), calls=%async_computation.2 | async-start | bytes 1048576 | tf_op jit(solution)/shard_map/all_to_all | solution.py:325
  56.7 0.9 reshape.108
  57.7 1.2 slice_add_fusion
  59.1 1.7 fusion.42
  60.7 7.8 %all-to-all-done.2.query_ref = bf16[32,32,256]{2,1,0:T(8,128)(2,1)S(1)} async-done(((bf16[32,32,256]{2,1,0:T(8,128)(2,1)}), bf16[32,32,256]{2,1,0:T(8,128)(2,1)S(1)}, u32[]{:S(2)}, u32[]{:S(2)}) %all-to-all-start.2) | async-done | bytes 524320 | tf_op jit(solution)/shard_map/all_to_all | solution.py:325
  68.5 31.1 %attend.1 = bf16[32,32,256]{2,1,0:T(8,128)(2,1)} custom-call(s32[1]{0:T(128)} %bitcast.6.boundary_ref, bf16[32,32,256]{2,1,0:T(8,128)(2,1)S(1)} %all-to-all-done.2.query_ref, bf16[8,4,288,128]{3,2,1,0:T(8,128)(2,1)S(1)} %all-to-all-done.1.kv_ref, f32[8,4,1,1024]{3,2,1,0:T(1,128)S(1)} %reshape_transpose_reshape.3.gate_ref), custom_call_target="tpu_custom_call" | custom-call | tf_op jit(solution)/shard_map/attend/pallas_call | solution.py:333
  99.6 6.3 %all-to-all-start.3 = ((bf16[32,32,256]{2,1,0:T(8,128)(2,1)}), bf16[32,32,256]{2,1,0:T(8,128)(2,1)S(1)}, u32[]{:S(2)}, u32[]{:S(2)}) async-start(bf16[32,32,256]{2,1,0:T(8,128)(2,1)} %attend.1), calls=%async_computation.3 | async-start | bytes 1048576 | tf_op jit(solution)/shard_map/all_to_all | solution.py:347
  106.1 1.2 reduce-window.6
  107.3 0.2 slice_reduce_fusion
  107.9 10.3 %all-to-all-done.3 = bf16[32,32,256]{2,1,0:T(8,128)(2,1)S(1)} async-done(((bf16[32,32,256]{2,1,0:T(8,128)(2,1)}), bf16[32,32,256]{2,1,0:T(8,128)(2,1)S(1)}, u32[]{:S(2)}, u32[]{:S(2)}) %all-to-all-start.3) | async-done | bytes 524320 | tf_op jit(solution)/shard_map/all_to_all | solution.py:347
  118.2 0.4 copy.77
  118.7 3.9 %fusion.13 = (f32[256]{0:T(256)S(1)}, bf16[256,2048]{1,0:T(8,128)(2,1)S(1)}) fusion(bf16[256,1024]{1,0:T(8,128)(2,1)S(1)} %bitcast.78, bf16[1024,2048]{1,0:T(8,128)(2,1)} %param.19, bf16[256,2048]{1,0:T(8,128)(2,1)} %param.18), kind=kOutput, calls=%fused_computation.16 | convolution fusion | flops 1076887296 | bytes 6816768 | tf_op jit(solution)/shard_map/dot_general | solution.py:353
  122.7 1.4 convolution_convert_fusion
  124.1 96.5 %all_to_all.31 = bf16[32,32,2048]{2,1,0:T(8,128)(2,1)S(1)} all-to-all(bf16[32,32,2048]{2,1,0:T(8,128)(2,1)S(1)} %bitcast.72), channel_id=1, replica_groups=mesh['sp'=32,'tp'=1] {'sp'}, dimensions={0} | all-to-all | bytes 8388608 | tf_op jit(solution)/shard_map/all_to_all | solution.py:373
  220.6 4.5 %fusion.2 = f32[1024,1024]{1,0:T(8,128)S(1)} fusion(bf16[1024,2048]{1,0:T(8,128)(2,1)S(1)} %bitcast.74, bf16[1,2048,1024]{2,1,0:T(8,128)(2,1)S(1)} %copy-done.4), kind=kOutput, calls=%fused_computation.2 | convolution fusion | flops 4294967296 | bytes 12582912 | tf_op jit(solution)/shard_map/dot_general | solution.py:377
  225.1 5.4 %multiply_convert_fusion = bf16[1024,1024]{1,0:T(8,128)(2,1)S(1)} fusion(f32[1024,1024]{1,0:T(8,128)S(1)} %fusion.2, bf16[1024,2048]{1,0:T(8,128)(2,1)S(1)} %bitcast.75, bf16[1,2048,1024]{2,1,0:T(8,128)(2,1)S(1)} %copy-done.5), kind=kOutput, calls=%fused_computation.6 | convolution fusion | flops 4301258752 | bytes 14680064 | tf_op jit(solution)/shard_map/dot_general | solution.py:376
  230.5 6.1 %fusion.6 = bf16[1024,2048]{1,0:T(8,128)(2,1)} fusion(bf16[1024,1024]{1,0:T(8,128)(2,1)S(1)} %multiply_convert_fusion, bf16[1,1024,2048]{2,1,0:T(8,128)(2,1)S(1)} %copy-done.6), kind=kOutput, calls=%fused_computation.8 | convolution fusion | flops 4297064448 | bytes 10485760 | tf_op jit(solution)/shard_map/dot_general | solution.py:379
  236.6 7.0 %all-to-all-start.5 = ((bf16[32,32,2048]{2,1,0:T(8,128)(2,1)}), bf16[32,32,2048]{2,1,0:T(8,128)(2,1)}, u32[]{:S(2)}, u32[]{:S(2)}) async-start(bf16[32,32,2048]{2,1,0:T(8,128)(2,1)} %bitcast.73), calls=%async_computation.5 | async-start | bytes 8388608 | tf_op jit(solution)/shard_map/all_to_all | solution.py:380
  243.6 90.0 %all-to-all-done.5 = bf16[32,32,2048]{2,1,0:T(8,128)(2,1)} async-done(((bf16[32,32,2048]{2,1,0:T(8,128)(2,1)}), bf16[32,32,2048]{2,1,0:T(8,128)(2,1)}, u32[]{:S(2)}, u32[]{:S(2)}) %all-to-all-start.5) | async-done | bytes 4194336 | tf_op jit(solution)/shard_map/all_to_all | solution.py:380
  333.6 3.6 %fusion.23 = f32[256,2048]{1,0:T(8,128)S(1)} fusion(bf16[1024,2048]{1,0:T(8,128)(2,1)} %bitcast.24, f32[256]{0:T(256)S(1)} %bitcast.91, s32[256]{0:T(256)S(1)} %bitcast.87, f32[256]{0:T(256)S(1)} %bitcast.89, s32[256]{0:T(256)S(1)} %bitcast.84), kind=kOutput, calls=%fused_computation.31 | convolution fusion | flops 1075576832 | bytes 6295552 | tf_op jit(solution)/shard_map/dot_general | solution.py:389
  337.3 4.7 %fusion.11 = bf16[256,2048]{1,0:T(8,128)(2,1)} fusion(f32[256,2048]{1,0:T(8,128)S(1)} %fusion.23, bf16[1024,2048]{1,0:T(8,128)(2,1)} %bitcast.24, bf16[256,2048]{1,0:T(8,128)(2,1)S(1)} %get-tuple-element.13, f32[256]{0:T(256)S(1)} %bitcast.92, s32[256]{0:T(256)S(1)} %bitcast.88, f32[256]{0:T(256)S(1)} %bitcast.90, s32[256]{0:T(256)S(1)} %bitcast.85), kind=kOutput, calls=%fused_computation.14 | convolution fusion | flops 1077936128 | bytes 8392704 | tf_op jit(solution)/shard_map/dot_general | solution.py:391
  (47 shorter events, 1.6 us)
Async XLA Ops:
  3.8 18.8 %copy-start = (bf16[256,1024]{1,0:T(8,128)(2,1)S(1)}, bf16[256,1024]{1,0:T(8,128)(2,1)}, u32[]{:S(2)}) copy-start(bf16[256,1024]{1,0:T(8,128)(2,1)} %param.13) | copy-start | bytes 1572868
  17.5 38.9 %copy-start.1 = (s32[256,2]{0,1:T(2,128)S(1)}, s32[256,2]{0,1:T(2,128)}, u32[]{:S(2)}) copy-start(s32[256,2]{0,1:T(2,128)} %param.21) | copy-start | bytes 6148
  17.5 33.0 %all-to-all-start.1 = ((bf16[8,4,288,128]{3,2,1,0:T(8,128)(2,1)}), bf16[8,4,288,128]{3,2,1,0:T(8,128)(2,1)S(1)}, u32[]{:S(2)}, u32[]{:S(2)}) async-start(bf16[8,4,288,128]{3,2,1,0:T(8,128)(2,1)} %broadcast_in_dim.42), calls=%async_computation.1 | async-start | bytes 4718592 | tf_op jit(solution)/shard_map/all_to_all | solution.py:314
  50.5 18.0 %all-to-all-start.2 = ((bf16[32,32,256]{2,1,0:T(8,128)(2,1)}), bf16[32,32,256]{2,1,0:T(8,128)(2,1)S(1)}, u32[]{:S(2)}, u32[]{:S(2)}) async-start(bf16[32,32,256]{2,1,0:T(8,128)(2,1)} %bitcast.8), calls=%async_computation.2 | async-start | bytes 1048576 | tf_op jit(solution)/shard_map/all_to_all | solution.py:325
  99.6 18.6 %all-to-all-start.3 = ((bf16[32,32,256]{2,1,0:T(8,128)(2,1)}), bf16[32,32,256]{2,1,0:T(8,128)(2,1)S(1)}, u32[]{:S(2)}, u32[]{:S(2)}) async-start(bf16[32,32,256]{2,1,0:T(8,128)(2,1)} %attend.1), calls=%async_computation.3 | async-start | bytes 1048576 | tf_op jit(solution)/shard_map/all_to_all | solution.py:347
  118.7 3.9 %copy-start.2 = (f32[2048]{0:T(1024)S(1)}, f32[2048]{0:T(1024)}, u32[]{:S(2)}) copy-start(f32[2048]{0:T(1024)} %param.20) | copy-start | bytes 24580
  124.1 96.5 %copy-start.4 = (bf16[1,2048,1024]{2,1,0:T(8,128)(2,1)S(1)}, bf16[1,2048,1024]{2,1,0:T(8,128)(2,1)}, u32[]{:S(2)}) copy-start(bf16[1,2048,1024]{2,1,0:T(8,128)(2,1)} %param.24) | copy-start | bytes 12582916
  220.6 4.5 %copy-start.5 = (bf16[1,2048,1024]{2,1,0:T(8,128)(2,1)S(1)}, bf16[1,2048,1024]{2,1,0:T(8,128)(2,1)}, u32[]{:S(2)}) copy-start(bf16[1,2048,1024]{2,1,0:T(8,128)(2,1)} %param.23) | copy-start | bytes 12582916
  225.1 5.4 %copy-start.6 = (bf16[1,1024,2048]{2,1,0:T(8,128)(2,1)S(1)}, bf16[1,1024,2048]{2,1,0:T(8,128)(2,1)}, u32[]{:S(2)}) copy-start(bf16[1,1024,2048]{2,1,0:T(8,128)(2,1)} %param.25) | copy-start | bytes 12582916
  236.6 7.0 %copy-start.3 = (f32[256,2]{0,1:T(2,128)S(1)}, f32[256,2]{0,1:T(2,128)}, u32[]{:S(2)}) copy-start(f32[256,2]{0,1:T(2,128)} %param.22) | copy-start | bytes 6148
  236.6 97.0 %all-to-all-start.5 = ((bf16[32,32,2048]{2,1,0:T(8,128)(2,1)}), bf16[32,32,2048]{2,1,0:T(8,128)(2,1)}, u32[]{:S(2)}, u32[]{:S(2)}) async-start(bf16[32,32,2048]{2,1,0:T(8,128)(2,1)} %bitcast.73), calls=%async_computation.5 | async-start | bytes 8388608 | tf_op jit(solution)/shard_map/all_to_all | solution.py:380
where the time goes:
time: 348 us; the launch traced here: 342 us
  waiting for transfers between devices  135 us (39%)
  blocking collectives  108 us (31%)
  Pallas kernels  31.1 us (9%)
  matrix products  29.6 us (9%)
  starting transfers between devices  24.3 us (7%)
  local copies, waits for them, and re-layouts  8.1 us (2%)
  other arithmetic  5.76 us (2%)
    all_to_all x1, blocking collectives, fast_shards(): lax.all_to_all(outgoing.reshape(experts_total, capacity, -1), 'sp', split...  96.5 us
    all_to_all x1, waiting for transfers between devices, fast_shards(): lax.all_to_all(answer.reshape(sp_count, capacity, -1), 'sp', split_axis=0...  90 us
    pallas_call x1, Pallas kernels, fast_shards(): pl.pallas_call(functools.partial(attend_kernel, sub, span, width), grid=(...  31.1 us
    all_to_all x1, waiting for transfers between devices, fast_shards(): lax.all_to_all(jnp.broadcast_to(column[None], (stripes,) + column.shape),...  26.6 us
    all_to_all x1, blocking collectives, fast_shards(): lax.all_to_all(message, 'sp', split_axis=0, concat_axis=0, axis_index_gro...  11.6 us
    all_to_all x1, waiting for transfers between devices, fast_shards(): back = lax.all_to_all(mixed, 'sp', split_axis=0, concat_axis=0, tiled=True)  10.3 us
    all_to_all x1, waiting for transfers between devices, fast_shards(): lax.all_to_all(query_send, 'sp', split_axis=0, concat_axis=0, tiled=True)  7.75 us
    all_to_all x1, starting transfers between devices, fast_shards(): lax.all_to_all(answer.reshape(sp_count, capacity, -1), 'sp', split_axis=0...  6.99 us
  transfers between devices with their start and end apart: 4, of which 4 were waited for; matrix products, arithmetic and copies ran while one was open for 2% of the time, Pallas kernels for 0%

commit v1 on v0

--- a/solution.py
+++ b/solution.py
@@ -266,6 +266,143 @@
     ratio = mixed[:, HD:] / mixed[:, :HD]
     parts = [ratio[head * rows:(head + 1) * rows] for head in range(group)]
     out_ref[...] = jnp.concatenate(parts, axis=1).astype(jnp.bfloat16).reshape(out_ref.shape)
+
+
+def exchange_kernel(
+    stripes, kv_ref, query_ref, kv_all_ref, got_ref, z_send, z_recv, p_send, p_recv, s_send, s_recv, q_send, q_recv
+):
+    total = query_ref.shape[0]
+    planes = total // stripes
+    chips = stripes // 2
+    me = lax.axis_index("sp")
+    plane, spot = me // stripes, lax.rem(me, stripes)
+    chip, core = spot // 2, lax.rem(spot, 2)
+    partner = plane * stripes + chip * 2 + (1 - core)
+    barrier = pltpu.get_barrier_semaphore()
+
+    def greet(r, carry):
+        pl.semaphore_signal(barrier, inc=1, device_id={"sp": lax.rem(me + r, total)})
+        return carry
+
+    lax.fori_loop(1, total, greet, 0)
+    pl.semaphore_wait(barrier, total - 1)
+
+    def along(r):
+        other = lax.rem(plane + r, planes)
+        return pltpu.make_async_remote_copy(
+            src_ref=kv_ref.at[other],
+            dst_ref=kv_all_ref.at[spot, plane],
+            send_sem=z_send.at[r],
+            recv_sem=z_recv.at[r],
+            device_id={"sp": other * stripes + spot},
+        )
+
+    def block(r):
+        if r == 0:
+            return kv_ref.at[plane]
+        return kv_all_ref.at[spot, lax.rem(plane + planes - r, planes)]
+
+    def across(r, m):
+        target = lax.rem(chip + m, chips)
+        return pltpu.make_async_remote_copy(
+            src_ref=block(r),
+            dst_ref=kv_all_ref.at[spot, lax.rem(plane + planes - r, planes)],
+            send_sem=p_send.at[r, m],
+            recv_sem=p_recv.at[r, m],
+            device_id={"sp": plane * stripes + target * 2 + core},
+        )
+
+    def over(r, m):
+        source = lax.rem(chip + chips - m, chips) * 2 + core
+        where = kv_all_ref.at[source, lax.rem(plane + planes - r, planes)]
+        return pltpu.make_async_remote_copy(
+            src_ref=block(r) if m == 0 else where,
+            dst_ref=where,
+            send_sem=s_send.at[r, m],
+            recv_sem=s_recv.at[r, m],
+            device_id={"sp": partner},
+        )
+
+    def direct(r):
+        other = lax.rem(me + r, total)
+        return pltpu.make_async_remote_copy(
+            src_ref=query_ref.at[other],
+            dst_ref=got_ref.at[me],
+            send_sem=q_send.at[r],
+            recv_sem=q_recv.at[r],
+            device_id={"sp": other},
+        )
+
+    order = sorted(range(1, planes), key=lambda r: min(r, planes - r))
+    for r in order:
+        along(r).start()
+    for m in range(1, chips):
+        across(0, m).start()
+    over(0, 0).start()
+
+    def send_query(r, carry):
+        direct(r).start()
+        return carry
+
+    lax.fori_loop(1, total, send_query, 0)
+    kv_all_ref[spot, plane] = kv_ref[plane]
+    got_ref[me] = query_ref[me]
+    for at, r in enumerate(order):
+        along(r).wait_recv()
+        for m in range(1, chips):
+            across(r, m).start()
+        over(r, 0).start()
+        earlier = 0 if at == 0 else order[at - 1]
+        for m in range(1, chips):
+            across(earlier, m).wait_recv()
+            over(earlier, m).start()
+    for m in range(1, chips):
+        across(order[-1], m).wait_recv()
+        over(order[-1], m).start()
+    for r in range(planes):
+        for m in range(chips):
+            over(r, m).wait()
+    for r in range(1, planes):
+        along(r).wait_send()
+    for r in range(planes):
+        for m in range(1, chips):
+            across(r, m).wait_send()
+
+    def end_query(r, carry):
+        direct(r).wait()
+        return carry
+
+    lax.fori_loop(1, total, end_query, 0)
+
+
+def exchange(message, query_send, stripes):
+    total = query_send.shape[0]
+    planes, chips = total // stripes, stripes // 2
+    vmem = pl.BlockSpec(memory_space=pltpu.VMEM)
+    dma = pltpu.SemaphoreType.DMA
+    return pl.pallas_call(
+        functools.partial(exchange_kernel, stripes),
+        in_specs=[vmem, vmem],
+        out_specs=[vmem, vmem],
+        out_shape=[
+            jax.ShapeDtypeStruct((stripes,) + message.shape, message.dtype),
+            jax.ShapeDtypeStruct(query_send.shape, query_send.dtype),
+        ],
+        scratch_shapes=[
+            dma((planes,)),
+            dma((planes,)),
+            dma((planes, chips)),
+            dma((planes, chips)),
+            dma((planes, chips)),
+            dma((planes, chips)),
+            dma((total,)),
+            dma((total,)),
+        ],
+        compiler_params=pltpu.CompilerParams(
+            collective_id=0, has_side_effects=True, vmem_limit_bytes=24 * 1024 * 1024
+        ),
+        name="exchange",
+    )(message, query_send)
 
 
 def fast_shards(
@@ -306,23 +443,10 @@
         [keys.reshape(tok, KV_HEADS, HD), values.reshape(tok, KV_HEADS, HD)], axis=2
     )
     message = jnp.concatenate([jnp.transpose(kv, (1, 0, 2)), extra], axis=1)
-    across = [[g * stripes + j for g in range(KV_HEADS)] for j in range(stripes)]
-    within = [[g * stripes + j for j in range(stripes)] for g in range(KV_HEADS)]
-    column = lax.all_to_all(
-        message, "sp", split_axis=0, concat_axis=0, axis_index_groups=across, tiled=True
-    )
-    kv_all = lax.all_to_all(
-        jnp.broadcast_to(column[None], (stripes,) + column.shape),
-        "sp",
-        split_axis=0,
-        concat_axis=0,
-        axis_index_groups=within,
-        tiled=True,
-    )
     query_send = jnp.transpose(
         queries.reshape(stripes, sub, KV_HEADS, group * HD), (2, 0, 1, 3)
     ).reshape(sp_count, sub, group * HD)
-    query_got = lax.all_to_all(query_send, "sp", split_axis=0, concat_axis=0, tiled=True)
+    kv_all, query_got = exchange(message, query_send, stripes)
     extra_all = jnp.transpose(kv_all[:, :, tok:, :], (1, 0, 2, 3)).reshape(sp_count, 16, tok)
     extra_all = extra_all.astype(jnp.float32)
     boundary = jnp.sum((extra_all[:, 3 * group, :] < 0.5).astype(jnp.int32)).reshape(1)
@@ -394,7 +518,7 @@
 
 def solution(mesh):
     sp_count, tp_count = mesh.shape["sp"], mesh.shape["tp"]
-    fast = tp_count == 1 and sp_count % 32 == 0
+    fast = tp_count == 1 and sp_count % (2 * KV_HEADS) == 0
     return jax.shard_map(
         fast_shards if fast else shards,
         mesh=mesh,

time: 348 us -> 314 us (0.902)
  waiting for transfers between devices: 135 us -> 100 us
  Pallas kernels: 31.1 us -> 59.5 us
  starting transfers between devices: 24.3 us -> 11.9 us
  blocking collectives: 108 us -> 96.5 us
    all_to_all x2 -> x0, waiting for transfers between devices: 34.3 us -> none  [the longest x1 26.6 us: fast_shards(): lax.all_to_all(jnp.broadcast_to(column[None], (stripes,) + column.shape),...]
    pallas_call x0 -> x1, Pallas kernels: none -> 26.4 us  [exchange(): pl.pallas_call(functools.partial(exchange_kernel, stripes), in_specs=[vme...]
    all_to_all x1 -> x0, blocking collectives: 11.6 us -> none  [fast_shards(): lax.all_to_all(message, 'sp', split_axis=0, concat_axis=0, axis_index_gro...]
    all_to_all x2 -> x0, starting transfers between devices: 11 us -> none  [the longest x1 5.81 us: fast_shards(): lax.all_to_all(query_send, 'sp', split_axis=0, concat_axis=0, tiled=True)]
  transfers between devices with their start and end apart: 4 -> 2, of which waited for: 4 -> 2; matrix products, arithmetic and copies ran while one was open for 2% -> 1% of each run, Pallas kernels for 0% -> 0%
where the time goes in v1:
time: 314 us; the launch traced here: 310 us
  waiting for transfers between devices  100 us (32%)
  blocking collectives  96.5 us (31%)
  Pallas kernels  59.5 us (19%)
  matrix products  29.6 us (9%)
  starting transfers between devices  11.9 us (4%)
  local copies, waits for them, and re-layouts  6.53 us (2%)
  other arithmetic  5.92 us (2%)
    all_to_all x1, blocking collectives, fast_shards(): lax.all_to_all(outgoing.reshape(experts_total, capacity, -1), 'sp', split...  96.5 us
    all_to_all x1, waiting for transfers between devices, fast_shards(): lax.all_to_all(answer.reshape(sp_count, capacity, -1), 'sp', split_axis=0...  90 us
    pallas_call x1, Pallas kernels, fast_shards(): pl.pallas_call(functools.partial(attend_kernel, sub, span, width), grid=(...  33.1 us
    pallas_call x1, Pallas kernels, exchange(): pl.pallas_call(functools.partial(exchange_kernel, stripes), in_specs=[vme...  26.4 us
    all_to_all x1, waiting for transfers between devices, fast_shards(): back = lax.all_to_all(mixed, 'sp', split_axis=0, concat_axis=0, tiled=True)  9.97 us
    all_to_all x1, starting transfers between devices, fast_shards(): lax.all_to_all(answer.reshape(sp_count, capacity, -1), 'sp', split_axis=0...  6.99 us
  transfers between devices with their start and end apart: 2, of which 2 were waited for; matrix products, arithmetic and copies ran while one was open for 1% of the time, Pallas kernels for 0%

profile of v1, /device:TPU:19, one launch (start us, length us, event | category | flops | bytes accessed | tf_op | source)
XLA Modules:
  0.0 310.3 jit_solution(16967740445517139172)
XLA Ops:
  0.0 0.7 reduce-precision_convert_fusion.3
  0.8 0.7 convert_element_type.60
  1.6 1.0 copy.50
  2.6 0.2 copy.52
  2.8 1.0 copy.51
  3.8 0.2 copy.53
  4.0 1.4 reshape.96
  5.5 0.1 maximum_bitcast_fusion
  5.7 26.4 %exchange.1 = (bf16[8,4,288,128]{3,2,1,0:T(8,128)(2,1)S(1)}, bf16[32,32,256]{2,1,0:T(8,128)(2,1)S(1)}) custom-call(bf16[4,288,128]{2,1,0:T(8,128)(2,1)S(1)} %pad_maximum_fusion.kv_ref, bf16[32,32,256]{2,1,0:T(8,128)(2,1)S(1)} %bitcast.72), custom_call_target="tpu_custom_call" | custom-call | tf_op jit(solution)/shard_map/exchange/pallas_call | solution.py:383
  32.2 0.9 reshape.107
  33.2 1.2 slice_add_fusion
  34.3 1.7 fusion.42
  36.1 0.2 reshape_transpose_reshape.3.gate_ref
  36.3 33.1 %attend.1 = bf16[32,32,256]{2,1,0:T(8,128)(2,1)} custom-call(s32[1]{0:T(128)} %bitcast.8.boundary_ref, bf16[32,32,256]{2,1,0:T(8,128)(2,1)S(1)} %get-tuple-element.8.query_ref, bf16[8,4,288,128]{3,2,1,0:T(8,128)(2,1)S(1)} %get-tuple-element.7.kv_ref, f32[8,4,1,1024]{3,2,1,0:T(1,128)S(1)} %reshape_transpose_reshape.3.gate_ref), custom_call_target="tpu_custom_call" | custom-call | tf_op jit(solution)/shard_map/attend/pallas_call | solution.py:457
  69.4 4.9 %all-to-all-start = ((bf16[32,32,256]{2,1,0:T(8,128)(2,1)}), bf16[32,32,256]{2,1,0:T(8,128)(2,1)S(1)}, u32[]{:S(2)}, u32[]{:S(2)}) async-start(bf16[32,32,256]{2,1,0:T(8,128)(2,1)} %attend.1), calls=%async_computation | async-start | bytes 1048576 | tf_op jit(solution)/shard_map/all_to_all | solution.py:471
  74.5 0.1 eq.86
  74.6 0.1 eq.82
  74.8 1.2 reduce-window.6
  75.9 0.2 slice_reduce_fusion
  76.3 0.1 sub.18
  76.6 10.0 %all-to-all-done = bf16[32,32,256]{2,1,0:T(8,128)(2,1)S(1)} async-done(((bf16[32,32,256]{2,1,0:T(8,128)(2,1)}), bf16[32,32,256]{2,1,0:T(8,128)(2,1)S(1)}, u32[]{:S(2)}, u32[]{:S(2)}) %all-to-all-start) | async-done | bytes 524320 | tf_op jit(solution)/shard_map/all_to_all | solution.py:471
  86.5 0.4 copy.61
  87.1 3.9 %fusion.13 = (f32[256]{0:T(256)S(1)}, bf16[256,2048]{1,0:T(8,128)(2,1)S(1)}) fusion(bf16[256,1024]{1,0:T(8,128)(2,1)S(1)} %bitcast.81, bf16[1024,2048]{1,0:T(8,128)(2,1)} %param.19, bf16[256,2048]{1,0:T(8,128)(2,1)} %param.18), kind=kOutput, calls=%fused_computation.16 | convolution fusion | flops 1076887296 | bytes 6816768 | tf_op jit(solution)/shard_map/dot_general | solution.py:477
  91.0 1.4 convolution_convert_fusion
  92.4 96.5 %all_to_all.15 = bf16[32,32,2048]{2,1,0:T(8,128)(2,1)S(1)} all-to-all(bf16[32,32,2048]{2,1,0:T(8,128)(2,1)S(1)} %bitcast.73), channel_id=1, replica_groups=mesh['sp'=32,'tp'=1] {'sp'}, dimensions={0} | all-to-all | bytes 8388608 | tf_op jit(solution)/shard_map/all_to_all | solution.py:497
  189.0 4.5 %fusion.2 = f32[1024,1024]{1,0:T(8,128)S(1)} fusion(bf16[1024,2048]{1,0:T(8,128)(2,1)S(1)} %bitcast.75, bf16[1,2048,1024]{2,1,0:T(8,128)(2,1)S(1)} %copy-done.3), kind=kOutput, calls=%fused_computation.2 | convolution fusion | flops 4294967296 | bytes 12582912 | tf_op jit(solution)/shard_map/dot_general | solution.py:501
  193.5 5.4 %multiply_convert_fusion = bf16[1024,1024]{1,0:T(8,128)(2,1)S(1)} fusion(f32[1024,1024]{1,0:T(8,128)S(1)} %fusion.2, bf16[1024,2048]{1,0:T(8,128)(2,1)S(1)} %bitcast.76, bf16[1,2048,1024]{2,1,0:T(8,128)(2,1)S(1)} %copy-done.4), kind=kOutput, calls=%fused_computation.6 | convolution fusion | flops 4301258752 | bytes 14680064 | tf_op jit(solution)/shard_map/dot_general | solution.py:500
  198.8 6.1 %fusion.6 = bf16[1024,2048]{1,0:T(8,128)(2,1)} fusion(bf16[1024,1024]{1,0:T(8,128)(2,1)S(1)} %multiply_convert_fusion, bf16[1,1024,2048]{2,1,0:T(8,128)(2,1)S(1)} %copy-done.5), kind=kOutput, calls=%fused_computation.8 | convolution fusion | flops 4297064448 | bytes 10485760 | tf_op jit(solution)/shard_map/dot_general | solution.py:503
  205.0 7.0 %all-to-all-start.2 = ((bf16[32,32,2048]{2,1,0:T(8,128)(2,1)}), bf16[32,32,2048]{2,1,0:T(8,128)(2,1)}, u32[]{:S(2)}, u32[]{:S(2)}) async-start(bf16[32,32,2048]{2,1,0:T(8,128)(2,1)} %bitcast.74), calls=%async_computation.2 | async-start | bytes 8388608 | tf_op jit(solution)/shard_map/all_to_all | solution.py:504
  212.0 90.0 %all-to-all-done.2 = bf16[32,32,2048]{2,1,0:T(8,128)(2,1)} async-done(((bf16[32,32,2048]{2,1,0:T(8,128)(2,1)}), bf16[32,32,2048]{2,1,0:T(8,128)(2,1)}, u32[]{:S(2)}, u32[]{:S(2)}) %all-to-all-start.2) | async-done | bytes 4194336 | tf_op jit(solution)/shard_map/all_to_all | solution.py:504
  302.0 3.6 %fusion.23 = f32[256,2048]{1,0:T(8,128)S(1)} fusion(bf16[1024,2048]{1,0:T(8,128)(2,1)} %bitcast.24, f32[256]{0:T(256)S(1)} %bitcast.92, s32[256]{0:T(256)S(1)} %bitcast.88, f32[256]{0:T(256)S(1)} %bitcast.90, s32[256]{0:T(256)S(1)} %bitcast.85), kind=kOutput, calls=%fused_computation.31 | convolution fusion | flops 1075576832 | bytes 6295552 | tf_op jit(solution)/shard_map/dot_general | solution.py:513
  305.6 4.7 %fusion.11 = bf16[256,2048]{1,0:T(8,128)(2,1)} fusion(f32[256,2048]{1,0:T(8,128)S(1)} %fusion.23, bf16[1024,2048]{1,0:T(8,128)(2,1)} %bitcast.24, bf16[256,2048]{1,0:T(8,128)(2,1)S(1)} %get-tuple-element.17, f32[256]{0:T(256)S(1)} %bitcast.93, s32[256]{0:T(256)S(1)} %bitcast.89, f32[256]{0:T(256)S(1)} %bitcast.91, s32[256]{0:T(256)S(1)} %bitcast.86), kind=kOutput, calls=%fused_computation.14 | convolution fusion | flops 1077936128 | bytes 8392704 | tf_op jit(solution)/shard_map/dot_general | solution.py:515
  (40 shorter events, 0.9 us)
Async XLA Ops:
  32.1 42.2 %copy-start = (s32[256,2]{0,1:T(2,128)S(1)}, s32[256,2]{0,1:T(2,128)}, u32[]{:S(2)}) copy-start(s32[256,2]{0,1:T(2,128)} %param.21) | copy-start | bytes 6148
  69.4 17.1 %all-to-all-start = ((bf16[32,32,256]{2,1,0:T(8,128)(2,1)}), bf16[32,32,256]{2,1,0:T(8,128)(2,1)S(1)}, u32[]{:S(2)}, u32[]{:S(2)}) async-start(bf16[32,32,256]{2,1,0:T(8,128)(2,1)} %attend.1), calls=%async_computation | async-start | bytes 1048576 | tf_op jit(solution)/shard_map/all_to_all | solution.py:471
  87.0 3.9 %copy-start.1 = (f32[2048]{0:T(1024)S(1)}, f32[2048]{0:T(1024)}, u32[]{:S(2)}) copy-start(f32[2048]{0:T(1024)} %param.20) | copy-start | bytes 24580
  92.4 96.5 %copy-start.3 = (bf16[1,2048,1024]{2,1,0:T(8,128)(2,1)S(1)}, bf16[1,2048,1024]{2,1,0:T(8,128)(2,1)}, u32[]{:S(2)}) copy-start(bf16[1,2048,1024]{2,1,0:T(8,128)(2,1)} %param.24) | copy-start | bytes 12582916
  188.9 4.5 %copy-start.4 = (bf16[1,2048,1024]{2,1,0:T(8,128)(2,1)S(1)}, bf16[1,2048,1024]{2,1,0:T(8,128)(2,1)}, u32[]{:S(2)}) copy-start(bf16[1,2048,1024]{2,1,0:T(8,128)(2,1)} %param.23) | copy-start | bytes 12582916
  193.5 5.4 %copy-start.5 = (bf16[1,1024,2048]{2,1,0:T(8,128)(2,1)S(1)}, bf16[1,1024,2048]{2,1,0:T(8,128)(2,1)}, u32[]{:S(2)}) copy-start(bf16[1,1024,2048]{2,1,0:T(8,128)(2,1)} %param.25) | copy-start | bytes 12582916
  204.9 7.0 %copy-start.2 = (f32[256,2]{0,1:T(2,128)S(1)}, f32[256,2]{0,1:T(2,128)}, u32[]{:S(2)}) copy-start(f32[256,2]{0,1:T(2,128)} %param.22) | copy-start | bytes 6148
  205.0 97.0 %all-to-all-start.2 = ((bf16[32,32,2048]{2,1,0:T(8,128)(2,1)}), bf16[32,32,2048]{2,1,0:T(8,128)(2,1)}, u32[]{:S(2)}, u32[]{:S(2)}) async-start(bf16[32,32,2048]{2,1,0:T(8,128)(2,1)} %bitcast.74), calls=%async_computation.2 | async-start | bytes 8388608 | tf_op jit(solution)/shard_map/all_to_all | solution.py:504
